TPU v7x, 32 devices: a whole 2x2x4 slice. The times are simulated.
32 devices in a mesh: ep: 8 (over z, y), tp: 4 (over x, core).
Axes of the slice: x: 2, y: 2, z: 4, core: 2. Of those that a mesh axis runs over, the one named last changes fastest.
Arguments:
- state_probe_logits: bfloat16 [8192, 1024], P('ep', 'tp'), may hold values from -6 to 6
- retention_logits: bfloat16 [8192, 1024], P('ep', 'tp'), may hold values from -12 to 12
- state_source_entries: bfloat16 [8192, 1024], P('ep', 'tp'), may hold values from -6 to 6
- state_result_switch_logits: bfloat16 [8192, 1024], P('ep', 'tp'), may hold values from -6 to 6
- retention_bound_margin: float32 [1024], P('tp'), may hold values from 0 to 0.07
- extra_fading_amount: float32 [8192, 8], P('ep', 'tp'), may hold values from -0.7 to 0
- state_result_scale: float32 [1024], P('tp'), may hold values from 0.1 to 1.9
- state_result_matrix: bfloat16 [1024, 2048], P(None, 'tp'), may hold values from -0.1875 to 0.1875
- second_slice_tokens: bfloat16 [4096, 2048], P('ep'), may hold values from -6 to 6
- specialist_assignment: int32 [4096, 2], P('ep'), may hold values from 0 to 7, all different within a row; in each aligned block of 128 rows (0 to 127, 128 to 255, ...) at most 64 rows name the same one
- selected_specialist_share: float32 [4096, 2], P('ep'), may hold values from 0.1 to 1
- leading_scale_vector: float32 [2048], replicated, may hold values from 0.1 to 1.9
- trailing_scale_vector: float32 [2048], replicated, may hold values from 0.1 to 1.9
- specialist_switch_matrix: bfloat16 [8, 2048, 2048], P('ep', None, 'tp'), may hold values from -0.3125 to 0.3125
- specialist_widen_matrix: bfloat16 [8, 2048, 2048], P('ep', None, 'tp'), may hold values from -0.3125 to 0.3125
- specialist_contract_matrix: bfloat16 [8, 2048, 2048], P('ep', 'tp'), may hold values from -0.125 to 0.125
Outputs:
- mixer_out: bfloat16 [8192, 2048], P('ep', 'tp')
- moe_out: bfloat16 [4096, 2048], P(('ep', 'tp'))
Inputs may be any that keep to these rules, and one draw needn't show every extreme that they name: `specialist_assignment`: each row names 2 different experts. In each aligned block of 128 rows no expert is named by more than 64 rows, a bound that some block reaches.
All inputs are finite; a program needn't handle non-finite values.
Results may differ from a plain program's by a relative error of at most 0.012.
Values may be sent and summed in bfloat16 or wider, within the bound.
A program may use at most 128 MiB of HBM per device.

v0:
```python
import jax
import jax.numpy as jnp
from jax import lax
from jax.sharding import PartitionSpec as P

HEAD = 128
SPAN_STEPS = 64
TOK_DEV = 128


NORM_EPS = 1e-06
SWISH_ALPHA = 1.702
CLAMP_LIMIT = 7.0
EXACT = lax.Precision.HIGHEST


def carried_in(shard, axis, join, neutral):
    place = lax.axis_index(axis)
    gathered = jax.tree.map(
        lambda a, kind: lax.all_gather(a.astype(kind), axis), shard, (jnp.bfloat16, jnp.bfloat16)
    )
    state = jax.tree.map(lambda a, e: jnp.zeros_like(a) + jnp.asarray(e, a.dtype), shard, neutral)

    def one(step, state):
        return join(
            state,
            jax.tree.map(
                lambda a, own: lax.dynamic_index_in_dim(a, step, 0, False).astype(own.dtype),
                gathered,
                shard,
            ),
        )

    return lax.fori_loop(0, place, one, state)


def rms_scale(values, gain):
    return values * lax.rsqrt(jnp.mean(values * values, axis=-1, keepdims=True) + NORM_EPS) * gain


def clamped_unit(gate, upward):
    glued = jnp.minimum(gate, CLAMP_LIMIT)
    linear = jnp.clip(upward, -CLAMP_LIMIT, CLAMP_LIMIT)
    return glued * jax.nn.sigmoid(SWISH_ALPHA * glued) * (linear + 1.0)


def slot_table(routes, quarters, experts, capacity):
    per_quarter = routes.shape[0] * routes.shape[1] // quarters
    flat = routes.reshape(quarters, per_quarter)
    onehot = (flat[:, :, None] == jnp.arange(experts, dtype=jnp.int32)[None, None, :]).astype(
        jnp.int32
    )
    rank = jnp.sum(onehot * (jnp.cumsum(onehot, axis=1) - 1), axis=2)
    quarter_ids = jnp.arange(quarters, dtype=jnp.int32)[:, None]
    return ((quarter_ids * experts + flat) * capacity + rank).reshape(-1)


def pack_rows(normed, routes, quarters, experts, capacity):
    slots = slot_table(routes, quarters, experts, capacity)
    room = quarters * experts * capacity
    owner = jnp.arange(slots.shape[0], dtype=jnp.int32) // routes.shape[1]
    source = jnp.zeros((room,), jnp.int32).at[slots].set(owner)
    filled = jnp.zeros((room,), jnp.bool_).at[slots].set(True)
    packed = jnp.where(filled[:, None], normed[source], jnp.zeros((), jnp.bfloat16))
    return packed.reshape(quarters, experts, capacity, normed.shape[1])


def shards(
    state_probe_logits,
    retention_logits,
    state_source_entries,
    state_result_switch_logits,
    retention_bound_margin,
    extra_fading_amount,
    state_result_scale,
    state_result_matrix,
    second_slice_tokens,
    specialist_assignment,
    selected_specialist_share,
    leading_scale_vector,
    trailing_scale_vector,
    specialist_switch_matrix,
    specialist_widen_matrix,
    specialist_contract_matrix,
):
    total_rows, width = state_probe_logits.shape
    groups_each_device = width // HEAD
    span_tally = total_rows // SPAN_STEPS

    def per_head(values):
        return values.reshape(span_tally, SPAN_STEPS, groups_each_device, HEAD).transpose(
            0, 2, 1, 3
        )

    query = per_head(jax.nn.silu(state_probe_logits.astype(jnp.float32)) * HEAD ** (-0.5))
    input_key = per_head(
        retention_bound_margin * jax.nn.sigmoid(-retention_logits.astype(jnp.float32))
    )
    decay_logarithm = (
        jnp.log1p(-input_key)
        + extra_fading_amount.reshape(span_tally, SPAN_STEPS, groups_each_device).transpose(
            0, 2, 1
        )[..., None]
    )
    values = per_head(state_source_entries.astype(jnp.float32))
    cumul = jnp.cumsum(decay_logarithm, axis=2)
    middle = cumul[:, :, SPAN_STEPS // 2 - 1 : SPAN_STEPS // 2]
    last = cumul[:, :, SPAN_STEPS - 1 :]
    causal = jnp.tril(jnp.ones((SPAN_STEPS, SPAN_STEPS), jnp.float32))
    scores = (
        jnp.einsum(
            "nhid,nhjd->nhij",
            query * jnp.exp(cumul - middle),
            input_key * jnp.exp(middle - cumul),
            precision=EXACT,
        )
        * causal
    )
    inner = jnp.einsum("nhij,nhje->nhie", scores, values, precision=EXACT)
    update = jnp.einsum(
        "nhcd,nhce->nhde", input_key * jnp.exp(last - cumul), values, precision=EXACT
    )
    block_decay = last[:, :, 0]

    def advance(state, operand_tensors):
        decay_log, addition = operand_tensors
        return (jnp.exp(decay_log)[..., None] * state + addition, state)

    end_state, local_start = lax.scan(
        advance, jnp.zeros((groups_each_device, HEAD, HEAD), jnp.float32), (block_decay, update)
    )
    decay_total = jnp.sum(block_decay, axis=0)
    running = jnp.cumsum(block_decay, axis=0)
    before = jnp.concatenate([jnp.zeros_like(running[:1]), running[:-1]], axis=0)

    def chain(earlier, later):
        return (earlier[0] + later[0], jnp.exp(later[0])[..., None] * earlier[1] + later[1])

    identity = (jnp.zeros_like(decay_total), jnp.zeros_like(end_state))
    entering = carried_in((decay_total, end_state), "ep", chain, identity)[1]
    start_state = local_start + jnp.exp(before)[..., None] * entering[None]
    outer = jnp.einsum("nhcd,nhde->nhce", query * jnp.exp(cumul), start_state, precision=EXACT)
    raw_out = inner + outer
    normed_rec = raw_out * lax.rsqrt(jnp.mean(raw_out * raw_out, axis=-1, keepdims=True) + NORM_EPS)
    normed_rec = normed_rec.transpose(0, 2, 1, 3).reshape(total_rows, width)
    state_layer_result = (
        normed_rec
        * state_result_scale
        * jax.nn.silu(state_result_switch_logits.astype(jnp.float32))
    ).astype(jnp.bfloat16)
    mixed = jnp.dot(
        lax.all_gather(state_layer_result, "tp", axis=1, tiled=True),
        state_result_matrix,
        preferred_element_type=jnp.float32,
    )
    mixer_out = mixed.astype(jnp.bfloat16)
    experts = specialist_switch_matrix.shape[0] * lax.axis_size("ep")
    top_count = specialist_assignment.shape[1]
    capacity = 2 * TOK_DEV * top_count // experts
    my_quarter = lax.axis_index("tp")
    own_route = lax.dynamic_slice_in_dim(specialist_assignment, my_quarter * TOK_DEV, TOK_DEV, 0)
    own_weight = lax.dynamic_slice_in_dim(
        selected_specialist_share, my_quarter * TOK_DEV, TOK_DEV, 0
    )
    own_rows = lax.dynamic_slice_in_dim(second_slice_tokens, my_quarter * TOK_DEV, TOK_DEV, 0)
    normed = rms_scale(own_rows.astype(jnp.float32), leading_scale_vector).astype(jnp.bfloat16)
    packed = pack_rows(normed, own_route, 1, experts, capacity)[0]
    arrived = lax.all_to_all(packed, "ep", split_axis=0, concat_axis=0, tiled=True)
    portion = lax.all_gather(arrived.reshape(-1, arrived.shape[2]), "tp", axis=0, tiled=True)
    gate = jnp.dot(portion, specialist_switch_matrix[0], preferred_element_type=jnp.float32)
    upward = jnp.dot(portion, specialist_widen_matrix[0], preferred_element_type=jnp.float32)
    activated = clamped_unit(gate, upward).astype(jnp.bfloat16)
    summed = lax.psum_scatter(
        jnp.dot(
            activated, specialist_contract_matrix[0], preferred_element_type=jnp.float32
        ).astype(jnp.bfloat16),
        "tp",
        scatter_dimension=0,
        tiled=True,
    ).astype(jnp.float32)
    finished = summed.astype(jnp.bfloat16).reshape(-1, capacity, summed.shape[1])
    returned = lax.all_to_all(finished, "ep", split_axis=0, concat_axis=0, tiled=True)
    flat_back = returned.reshape(-1, returned.shape[2])
    own_slots = slot_table(own_route, 1, experts, capacity).reshape(TOK_DEV, top_count)
    combined = jnp.zeros((TOK_DEV, flat_back.shape[1]), jnp.float32)
    for column in range(top_count):
        combined = (
            combined
            + flat_back[own_slots[:, column]].astype(jnp.float32)
            * own_weight[:, column : column + 1]
        )
    moe_out = rms_scale(combined, trailing_scale_vector).astype(jnp.bfloat16)
    return (mixer_out, moe_out)


def solution(mesh):
    return jax.shard_map(
        shards,
        mesh=mesh,
        in_specs=(
            P("ep", "tp"),
            P("ep", "tp"),
            P("ep", "tp"),
            P("ep", "tp"),
            P("tp"),
            P("ep", "tp"),
            P("tp"),
            P(None, "tp"),
            P("ep", None),
            P("ep", None),
            P("ep", None),
            P(),
            P(),
            P("ep", None, "tp"),
            P("ep", None, "tp"),
            P("ep", "tp", None),
        ),
        out_specs=(P("ep", "tp"), P(("ep", "tp"), None)),
        check_vma=False,
    )
```

profile of v0, /device:TPU:0, one launch (start us, length us, event | category | flops | bytes accessed | tf_op | source)
XLA Modules:
  0.0 319.7 jit_solution(7436080060260765271)
XLA Ops:
  7.2 0.8 constant_dynamic-slice_fusion.1
  9.6 1.4 scatter_custom_fusion.1
  11.0 1.2 fusion.15
  12.3 1.5 scatter_custom_fusion
  13.9 1.2 fusion.17
  15.1 3.3 %gather_fusion = bf16[512,2048]{1,0:T(8,128)(2,1)} fusion(bf16[128,2048]{1,0:T(8,128)(2,1)S(1)} %fusion.17, s32[1024]{0:T(1024)S(1)} %pad_clamp_fusion.2), kind=kCustom, calls=%fused_computation | custom fusion | bytes 4196352 | tf_op jit(solution)/shard_map/gather | solution.py:64
  18.5 1.8 broadcast_select_fusion
  20.3 55.4 %all_to_all.10 = bf16[8,64,2048]{2,1,0:T(8,128)(2,1)} all-to-all(bf16[8,64,2048]{2,1,0:T(8,128)(2,1)S(1)} %broadcast_select_fusion), channel_id=1, replica_groups=mesh['ep'=8,'tp'=4] {'ep'}, dimensions={0} | all-to-all | bytes 4194304 | tf_op jit(solution)/shard_map/all_to_all | solution.py:168
  76.0 57.2 %all-gather.8.cloned.1.call-done = bf16[2048,2048]{1,0:T(8,128)(2,1)} async-done(((bf16[512,2048]{1,0:T(8,128)(2,1)}), bf16[2048,2048]{1,0:T(8,128)(2,1)}) %all-gather.8.cloned.1.call-update) | async-done | bytes 8388624 | tf_op jit(solution)/shard_map/all_gather | solution.py:169
  133.2 7.7 %fusion.2 = f32[2048,512]{1,0:T(8,128)S(1)} fusion(bf16[2048,2048]{1,0:T(8,128)(2,1)} %all-gather.8.cloned.1.call-done, bf16[1,2048,512]{2,1,0:T(8,128)(2,1)} %param.33), kind=kOutput, calls=%fused_computation.14 | convolution fusion | flops 4294967296 | bytes 14680064 | tf_op jit(solution)/shard_map/dot_general | solution.py:170
  140.9 5.6 %multiply_convert_fusion = bf16[2048,512]{1,0:T(8,128)(2,1)S(1)} fusion(f32[2048,512]{1,0:T(8,128)S(1)} %fusion.2, bf16[2048,2048]{1,0:T(8,128)(2,1)S(1)} %copy-done.12, bf16[1,2048,512]{2,1,0:T(8,128)(2,1)S(1)} %copy-done.13), kind=kOutput, calls=%fused_computation.11 | convolution fusion | flops 4305453056 | bytes 16777216 | tf_op jit(solution)/shard_map/dot_general | solution.py:171
  146.5 6.8 %convolution_convert_fusion = bf16[2048,2048]{1,0:T(8,128)(2,1)} fusion(bf16[2048,512]{1,0:T(8,128)(2,1)S(1)} %multiply_convert_fusion, bf16[1,512,2048]{2,1,0:T(8,128)(2,1)S(1)} %copy-done), kind=kOutput, calls=%fused_computation.10 | convolution fusion | flops 4299161600 | bytes 12582912 | tf_op jit(solution)/shard_map/dot_general | solution.py:174
  153.3 1.0 copy-done.7
  155.6 1.5 reshape.255
  157.1 1.2 reshape.258
  158.3 0.8 fusion.20
  159.8 2.8 bitcast_multiply_fusion.5
  162.6 3.4 %fusion.23 = f32[16,2,128,128]{3,2,1,0:T(8,128)} fusion(f32[16,2,64,128]{3,0,1,2:T(8,128)S(1)} %get-tuple-element.141, bf16[16,64,2,128]{3,2,1,0:T(2,128)(2,1)S(1)} %reshape.258), kind=kOutput, calls=%fused_computation.51 | convolution fusion | flops 402653184 | bytes 3670016 | tf_op jit(solution)/shard_map/nhcd,nhce->nhde/dot_general | solution.py:120
  166.0 27.6 %while.26 = (s32[]{:T(128)}, f32[2,128,128]{2,1,0:T(8,128)S(1)}, f32[16,2,128,128]{3,2,1,0:T(8,128)}, f32[16,2,128]{2,1,0:T(2,128)S(1)}, f32[16,2,128,128]{3,2,1,0:T(8,128)}, /*index=5*/s32[]{:T(128)}, s32[]{:T(128)}) while((s32[]{:T(128)}, f32[2,128,128]{2,1,0:T(8,128)S(1)}, f32[16,2,128,128]{3,2,1,0:T(8,128)}, ...), condition=%wide.region_2.3_spmd.clone, body=%wide.region_1.2_spmd.clone.sunk | while | flops 131075 | bytes 659040 | solution.py:129
  166.7 1.1 bitcast_add_fusion.3
  168.4 1.0 bitcast_add_fusion.3
  170.2 1.0 bitcast_add_fusion.3
  171.9 1.0 bitcast_add_fusion.3
  173.6 1.0 bitcast_add_fusion.3
  175.3 1.0 bitcast_add_fusion.3
  177.1 1.0 bitcast_add_fusion.3
  178.8 1.0 bitcast_add_fusion.3
  180.5 1.0 bitcast_add_fusion.3
  182.2 1.0 bitcast_add_fusion.3
  183.9 1.0 bitcast_add_fusion.3
  185.6 1.0 bitcast_add_fusion.3
  187.4 1.0 bitcast_add_fusion.3
  189.1 1.0 bitcast_add_fusion.3
  190.8 1.1 bitcast_add_fusion.3
  192.5 1.0 bitcast_add_fusion.3
  193.6 20.6 %all-gather.2 = bf16[8,2,128]{2,1,0:T(2,128)(2,1)S(1)} all-gather(bf16[1,2,128]{2,1,0:T(2,128)(2,1)S(1)} %bitcast.117), channel_id=2, replica_groups=mesh['ep'=8,'tp'=4] {'ep'}, dimensions={0}, use_global_device_ids=true | all-gather | bytes 4608 | tf_op jit(solution)/shard_map/all_gather | solution.py:20
  214.3 33.6 %all-gather.1 = bf16[16,128,128]{2,1,0:T(8,128)(2,1)} all-gather(bf16[2,128,128]{2,1,0:T(8,128)(2,1)S(1)} %convert_element_type.85), channel_id=3, replica_groups=mesh['ep'=8,'tp'=4] {'ep'}, dimensions={0}, use_global_device_ids=true | all-gather | bytes 589824 | tf_op jit(solution)/shard_map/all_gather | solution.py:20
  247.9 3.9 %convolution_multiply_fusion = f32[16,2,64,64]{3,2,1,0:T(8,128)} fusion(f32[16,2,64,128]{3,0,1,2:T(8,128)S(1)} %copy-done.3, f32[16,2,64,128]{3,0,1,2:T(8,128)S(1)} %get-tuple-element.137, f32[64,64]{1,0:T(8,128)S(1)} %fusion.38), kind=kOutput, calls=%fused_computation.22 | convolution fusion | flops 201457664 | bytes 2637824 | tf_op jit(solution)/shard_map/nhid,nhjd->nhij/dot_general | solution.py:111
  251.8 4.5 %fusion.4 = f32[16,2,64,128]{3,2,1,0:T(8,128)S(1)} fusion(f32[16,2,128,128]{3,2,1,0:T(8,128)} %get-tuple-element.74, f32[16,2,64,128]{3,0,1,2:T(8,128)} %get-tuple-element.138, f32[2,128,128]{2,1,0:T(8,128)S(1)} %get-tuple-element.76, f32[16,2,128]{2,1,0:T(2,128)S(1)} %pad_exponential_fusion), kind=kOutput, calls=%fused_computation.16 | convolution fusion | flops 403701760 | bytes 4341760 | tf_op jit(solution)/shard_map/nhcd,nhde->nhce/dot_general | solution.py:142
  256.4 1.0 multiply_reduce_fusion.1
  258.6 8.5 %all-to-all-start.1 = ((bf16[8,64,2048]{2,1,0:T(8,128)(2,1)}), bf16[8,64,2048]{2,1,0:T(8,128)(2,1)S(1)}, u32[]{:S(2)}, u32[]{:S(2)}) async-start(bf16[8,64,2048]{2,1,0:T(8,128)(2,1)} %bitcast.112), calls=%async_computation.2 | async-start | bytes 4194304 | tf_op jit(solution)/shard_map/all_to_all | solution.py:182
  267.1 2.2 fusion.29
  270.2 23.1 %all-gather.6.cloned.1.call-done = bf16[1024,1024]{1,0:T(8,128)(2,1)} async-done(((bf16[1024,256]{1,0:T(8,128)(2,1)}), bf16[1024,1024]{1,0:T(8,128)(2,1)}) %all-gather.6.cloned.1.call-update) | async-done | bytes 2097168 | tf_op jit(solution)/shard_map/all_gather | solution.py:152
  293.3 4.1 %convolution_convert_fusion.1 = bf16[1024,512]{1,0:T(8,128)(2,1)} fusion(bf16[1024,1024]{1,0:T(8,128)(2,1)} %all-gather.6.cloned.1.call-done, bf16[1024,512]{1,0:T(8,128)(2,1)} %param.27), kind=kOutput, calls=%fused_computation.20 | convolution fusion | flops 1074266112 | bytes 4194304 | tf_op jit(solution)/shard_map/dot_general | solution.py:151
  297.4 9.4 %all-to-all-done.1 = bf16[8,64,2048]{2,1,0:T(8,128)(2,1)S(1)} async-done(((bf16[8,64,2048]{2,1,0:T(8,128)(2,1)}), bf16[8,64,2048]{2,1,0:T(8,128)(2,1)S(1)}, u32[]{:S(2)}, u32[]{:S(2)}) %all-to-all-start.1) | async-done | bytes 2097184 | tf_op jit(solution)/shard_map/all_to_all | solution.py:182
  306.8 0.9 gather_fusion.1
  308.1 3.5 %gather_fusion.2 = bf16[128,2048]{1,0:T(8,128)(2,1)S(1)} fusion(bf16[512,2048]{1,0:T(8,128)(2,1)} %bitcast.108, s32[1024]{0:T(1024)S(1)} %get-tuple-element.152), kind=kCustom, calls=%fused_computation.2 | custom fusion | bytes 1049088 | tf_op jit(solution)/shard_map/gather | solution.py:189
  312.0 1.1 multiply_convert_fusion.1
  (109 shorter events, 17.5 us)
Async XLA Ops:
  7.2 139.3 %copy-start = (bf16[1,512,2048]{2,1,0:T(8,128)(2,1)S(1)}, bf16[1,512,2048]{2,1,0:T(8,128)(2,1)}, u32[]{:S(2)}) copy-start(bf16[1,512,2048]{2,1,0:T(8,128)(2,1)} %param.35) | copy-start | bytes 6291460
  7.2 126.0 %all-gather.8.cloned.1.call-start = ((), (), s32[]{:S(2)}) async-start(), calls=%async_computation.4 | async-start | bytes 10485760 | tf_op jit(solution)/shard_map/all_gather | solution.py:169
  75.7 182.8 %reduce-scatter.2.cloned.1.call-start = ((), (), s32[]{:S(2)}) async-start(), calls=%async_computation.5 | async-start | bytes 10485760 | tf_op jit(solution)/shard_map/reduce_scatter | solution.py:173
  133.2 7.7 %copy-start.12 = (bf16[2048,2048]{1,0:T(8,128)(2,1)S(1)}, bf16[2048,2048]{1,0:T(8,128)(2,1)}, u32[]{:S(2)}) copy-start(bf16[2048,2048]{1,0:T(8,128)(2,1)} %all-gather.8.cloned.1.call-done) | copy-start | bytes 25165828
  133.2 7.7 %copy-start.13 = (bf16[1,2048,512]{2,1,0:T(8,128)(2,1)S(1)}, bf16[1,2048,512]{2,1,0:T(8,128)(2,1)}, u32[]{:S(2)}) copy-start(bf16[1,2048,512]{2,1,0:T(8,128)(2,1)} %param.34) | copy-start | bytes 6291460
  153.3 1.0 copy-start.7
  153.3 1.0 copy-start.11
  153.3 1.9 copy-start.9
  153.3 2.0 copy-start.6
  158.3 1.5 copy-start.5
  166.0 81.9 %copy-start.3 = (f32[16,2,64,128]{3,0,1,2:T(8,128)S(1)}, f32[16,2,64,128]{3,0,1,2:T(8,128)}, u32[]{:S(2)}) copy-start(f32[16,2,64,128]{3,0,1,2:T(8,128)} %get-tuple-element.142) | copy-start | bytes 3145732
  251.8 4.5 %copy-start.4 = (f32[16,2,64,64]{3,2,1,0:T(8,128)S(1)}, f32[16,2,64,64]{3,2,1,0:T(8,128)}, u32[]{:S(2)}) copy-start(f32[16,2,64,64]{3,2,1,0:T(8,128)} %convolution_multiply_fusion) | copy-start | bytes 1572868
  258.5 8.5 %copy-start.10 = (f32[256]{0:T(256)S(1)}, f32[256]{0:T(256)}, u32[]{:S(2)}) copy-start(f32[256]{0:T(256)} %param.26) | copy-start | bytes 3076
  258.6 48.2 %all-to-all-start.1 = ((bf16[8,64,2048]{2,1,0:T(8,128)(2,1)}), bf16[8,64,2048]{2,1,0:T(8,128)(2,1)S(1)}, u32[]{:S(2)}, u32[]{:S(2)}) async-start(bf16[8,64,2048]{2,1,0:T(8,128)(2,1)} %bitcast.112), calls=%async_computation.2 | async-start | bytes 4194304 | tf_op jit(solution)/shard_map/all_to_all | solution.py:182
  267.0 26.3 %all-gather.6.cloned.1.call-start = ((), (), s32[]{:S(2)}) async-start(), calls=%async_computation.3 | async-start | bytes 2621440 | tf_op jit(solution)/shard_map/all_gather | solution.py:152
  306.8 1.4 copy-start.2
  308.1 3.9 %copy-start.8 = (f32[2048]{0:T(1024)S(1)}, f32[2048]{0:T(1024)}, u32[]{:S(2)}) copy-start(f32[2048]{0:T(1024)} %param.32) | copy-start | bytes 24580
  308.1 5.0 %copy-start.1 = (bf16[1,512,2048]{2,1,0:T(8,128)(2,1)S(1)}, bf16[1,512,2048]{2,1,0:T(8,128)(2,1)}, u32[]{:S(2)}) copy-start(bf16[1,512,2048]{2,1,0:T(8,128)(2,1)} %param.35) | copy-start | bytes 6291460
Sparse Core Ops, SparseCore 0:
  75.8 57.2 all-gather.7
  153.4 71.3 reduce-scatter.1
  270.0 23.2 all-gather.5
where the time goes:
time: 321 us; the launch traced here: 320 us
  blocking collectives  110 us (34%)
  waiting for transfers between devices  89.8 us (28%)
  other arithmetic  40.6 us (13%)
  matrix products  36.9 us (11%)
  local copies, waits for them, and re-layouts  19.3 us (6%)
  between operations  14.2 us (4%)
  starting transfers between devices  8.79 us (3%)
    all_gather x1, waiting for transfers between devices, shards(): lax.all_gather(arrived.reshape(-1, arrived.shape[2]), 'tp', axis=0, tiled...  57.2 us
    all_to_all x1, blocking collectives, shards(): lax.all_to_all(packed, 'ep', split_axis=0, concat_axis=0, tiled=True)  55.4 us
    all_gather x2, blocking collectives, carried_in(): lax.all_gather(a.astype(kind), axis)  54.2 us
    all_gather x1, waiting for transfers between devices, shards(): lax.all_gather(state_layer_result, 'tp', axis=1, tiled=True)  23.1 us
    add x16, other arithmetic, advance(): return (jnp.exp(decay_log)[..., None] * state + addition, state)  16.5 us
    dynamic_update_slice x16, other arithmetic, shards(): lax.scan(advance, jnp.zeros((groups_each_device, HEAD, HEAD), jnp.float32...  10.6 us
    all_to_all x1, waiting for transfers between devices, shards(): lax.all_to_all(finished, 'ep', split_axis=0, concat_axis=0, tiled=True)  9.41 us
    all_to_all x1, starting transfers between devices, shards(): lax.all_to_all(finished, 'ep', split_axis=0, concat_axis=0, tiled=True)  8.49 us
  transfers between devices with their start and end apart: 4, of which 3 were waited for; matrix products, arithmetic and copies ran while one was open for 17% of the time, Pallas kernels for 0%

commit v1 on v0

v1 whole, which is shorter than its diff:
```python
import functools

import jax
import jax.numpy as jnp
from jax import lax
from jax.experimental import pallas as pl
from jax.experimental.pallas import tpu as pltpu
from jax.sharding import PartitionSpec as P

HEAD = 128
SPAN = 128
TOK_DEV = 128

NORM_EPS = 1e-06
SWISH_ALPHA = 1.702
CLAMP_LIMIT = 7.0
MESH = pl.DeviceIdType.MESH
VMEM = pltpu.VMEM
DMA = pltpu.SemaphoreType.DMA
NT = (((1,), (1,)), ((), ()))
TN = (((0,), (0,)), ((), ()))


def xor(a, b, n):
    total, bit = 0, 1
    while bit < n:
        total = total + ((a // bit + b // bit) % 2) * bit
        bit *= 2
    return total


def places():
    i, j = lax.axis_index("ep"), lax.axis_index("tp")
    mate = j + 1 - 2 * (j % 2)
    cross = (j + 2) % 4
    return i, j, mate, cross


def greet(n, i, j, mate, cross):
    barrier = pltpu.get_barrier_semaphore()

    def one(s, c):
        pl.semaphore_signal(barrier, inc=1, device_id=((i + s) % n, j), device_id_type=MESH)
        return c

    lax.fori_loop(1, n, one, 0)
    for t in (mate, cross):
        pl.semaphore_signal(barrier, inc=1, device_id=(i, t), device_id_type=MESH)
    pl.semaphore_wait(barrier, n + 1)


def remote(src, dst, send, recv, where):
    return pltpu.make_async_remote_copy(
        src_ref=src, dst_ref=dst, send_sem=send, recv_sem=recv, device_id=where, device_id_type=MESH
    )


def span_step(t, probe, ret, val, margin, extra, raw, qdec, state, running):
    rows = pl.ds(pl.multiple_of(t * SPAN, SPAN), SPAN)
    width = probe.shape[1]
    x = probe[rows, :].astype(jnp.float32)
    q = x * jax.nn.sigmoid(x) * HEAD ** (-0.5)
    k = margin[...] * jax.nn.sigmoid(-ret[rows, :].astype(jnp.float32))
    logs = jnp.log1p(-k)
    row = lax.broadcasted_iota(jnp.int32, (SPAN, SPAN), 0)
    col = lax.broadcasted_iota(jnp.int32, (SPAN, SPAN), 1)
    causal = row >= col
    tril = jnp.where(causal, 1.0, 0.0).astype(jnp.float32)
    for h in range(width // HEAD):
        cols = slice(h * HEAD, (h + 1) * HEAD)
        qh, kh = q[:, cols], k[:, cols]
        ld = logs[:, cols] + extra[rows, h : h + 1]
        cum = jnp.dot(
            tril, ld, precision=lax.Precision.HIGHEST, preferred_element_type=jnp.float32
        )
        middle = cum[SPAN // 2 - 1 : SPAN // 2, :]
        last = cum[SPAN - 1 :, :]
        a = (qh * jnp.exp(cum - middle)).astype(jnp.bfloat16)
        b = (kh * jnp.exp(middle - cum)).astype(jnp.bfloat16)
        qe = qh * jnp.exp(cum)
        kd = (kh * jnp.exp(last - cum)).astype(jnp.bfloat16)
        v = val[rows, cols]
        s = lax.dot_general(a, b, NT, preferred_element_type=jnp.float32)
        s = jnp.where(causal, s, 0.0).astype(jnp.bfloat16)
        st = state[h]
        out = jnp.dot(s, v, preferred_element_type=jnp.float32)
        out = out + lax.dot_general(
            qe.astype(jnp.bfloat16), st.astype(jnp.bfloat16), NT, preferred_element_type=jnp.float32
        )
        raw[rows, cols] = out
        before = running[0:1, cols]
        qdec[rows, cols] = (qe * jnp.exp(before)).astype(jnp.bfloat16)
        state[h] = jnp.exp(last) * st + lax.dot_general(
            v, kd, TN, preferred_element_type=jnp.float32
        )
        running[:, cols] = running[:, cols] + last


def dispatch_kernel(
    n, packed, probe, ret, val, margin, extra,
    out, raw, qdec, state_out, running,
    state, asend, arecv, xsend, xrecv, csend, crecv, dsend, drecv, own_sem,
):
    i, j, mate, cross = places()
    spans = probe.shape[0] // SPAN
    greet(n, i, j, mate, cross)

    def direct(s):
        k = xor(i, s, n)
        return remote(packed.at[k], out.at[j, i], asend.at[s], arecv.at[s], (k, j))

    def over_x(src, s):
        k = xor(i, s, n)
        return remote(src, out.at[j, k], xsend.at[s], xrecv.at[s], (i, cross))

    def over_c(src, s):
        k = xor(i, s, n)
        return remote(src, out.at[j, k], csend.at[s], crecv.at[s], (i, mate))

    def over_d(s):
        k = xor(i, s, n)
        return remote(out.at[cross, k], out.at[cross, k], dsend.at[s], drecv.at[s], (i, mate))

    def start_direct(t, c):
        direct(n - 1 - t).start()
        return c

    lax.fori_loop(0, n - 1, start_direct, 0)
    own = pltpu.make_async_copy(packed.at[i], out.at[j, i], own_sem)
    own.start()
    over_x(packed.at[i], 0).start()
    over_c(packed.at[i], 0).start()
    state[...] = jnp.zeros_like(state)
    running[...] = jnp.zeros_like(running)

    def span(t):
        span_step(t, probe, ret, val, margin, extra, raw, qdec, state, running)

    def serve(t, c):
        @pl.when(t < spans)
        def _():
            span(t)

        s = n - 1 - t
        k = xor(i, s, n)
        direct(s).wait_recv()
        over_x(out.at[j, k], s).start()
        over_c(out.at[j, k], s).start()
        before = (s + 1) % n
        over_x(out.at[j, xor(i, before, n)], before).wait_recv()
        over_d(before).start()
        return c

    lax.fori_loop(0, n - 1, serve, 0)

    def rest(t, c):
        span(t)
        return c

    if spans > n - 1:
        lax.fori_loop(n - 1, spans, rest, 0)
    over_x(packed.at[i], 1).wait_recv()
    over_d(1).start()
    own.wait()

    def finish(s, c):
        over_x(packed.at[i], s).wait_send()
        over_c(packed.at[i], s).wait_send()
        over_c(packed.at[i], s).wait_recv()
        over_d(s).wait()
        return c

    lax.fori_loop(0, n, finish, 0)

    def finish_direct(s, c):
        direct(s).wait_send()
        return c

    lax.fori_loop(1, n, finish_direct, 0)
    for h in range(state.shape[0]):
        state_out[h] = state[h].astype(jnp.bfloat16)


def dispatch(n, packed, probe, ret, val, margin, extra):
    rows, width = probe.shape
    heads = width // HEAD
    vm = pl.BlockSpec(memory_space=VMEM)
    hbm = pl.BlockSpec(memory_space=pl.ANY)
    return pl.pallas_call(
        functools.partial(dispatch_kernel, n),
        name="dispatch",
        out_shape=(
            jax.ShapeDtypeStruct((4,) + packed.shape, jnp.bfloat16),
            jax.ShapeDtypeStruct((rows, width), jnp.float32),
            jax.ShapeDtypeStruct((rows, width), jnp.bfloat16),
            jax.ShapeDtypeStruct((heads, HEAD, HEAD), jnp.bfloat16),
            jax.ShapeDtypeStruct((8, width), jnp.float32),
        ),
        in_specs=[vm] * 6,
        out_specs=(hbm, vm, vm, vm, vm),
        scratch_shapes=[VMEM((heads, HEAD, HEAD), jnp.float32)] + [DMA((n,))] * 8 + [DMA],
        compiler_params=pltpu.CompilerParams(
            collective_id=0, has_side_effects=True, vmem_limit_bytes=48 * 2**20
        ),
        cost_estimate=pl.CostEstimate(
            flops=10**9, bytes_accessed=150 * 10**6, transcendentals=10**6
        ),
    )(packed, probe, ret, val, margin, extra)


def mixer_kernel(
    n, chunks, raw, qdec, switch, state, decay, scale, weight,
    out,
    states, decays, gath, enter, ssend, srecv, esend, erecv,
    xsend, xrecv, csend, crecv, dsend, drecv,
):
    i, j, mate, cross = places()
    rows, width = raw.shape
    part = rows // chunks
    heads = width // HEAD
    greet(n, i, j, mate, cross)

    def send_state(s):
        k = (i + s) % n
        return remote(state, states.at[i], ssend.at[s], srecv.at[s], (k, j))

    def send_decay(s):
        k = (i + s) % n
        return remote(decay, decays.at[i], esend.at[s], erecv.at[s], (k, j))

    def begin(s, c):
        send_state(s).start()
        send_decay(s).start()
        return c

    lax.fori_loop(1, n, begin, 0)

    def end(s, c):
        send_state(s).wait()
        send_decay(s).wait()
        return c

    lax.fori_loop(1, n, end, 0)
    enter[...] = jnp.zeros_like(enter)

    def join(p, c):
        @pl.when(p < i)
        def _():
            for h in range(heads):
                d = decays[p, 0:1, h * HEAD : (h + 1) * HEAD]
                enter[h] = jnp.exp(d) * enter[h] + states[p, h].astype(jnp.float32)

        return c

    lax.fori_loop(0, n, join, 0)

    def at(c):
        return pl.ds(pl.multiple_of(c * part, part), part)

    def over_x(c):
        here = gath.at[j, at(c)]
        return remote(here, here, xsend.at[c], xrecv.at[c], (i, cross))

    def over_c(c):
        here = gath.at[j, at(c)]
        return remote(here, here, csend.at[c], crecv.at[c], (i, mate))

    def over_d(c):
        here = gath.at[cross, at(c)]
        return remote(here, here, dsend.at[c], drecv.at[c], (i, mate))

    def final(c, carry):
        r = at(c)
        for h in range(heads):
            cols = slice(h * HEAD, (h + 1) * HEAD)
            x = raw[r, cols] + lax.dot_general(
                qdec[r, cols], enter[h].astype(jnp.bfloat16), NT,
                preferred_element_type=jnp.float32,
            )
            x = x * lax.rsqrt(jnp.mean(x * x, axis=-1, keepdims=True) + NORM_EPS)
            g = switch[r, cols].astype(jnp.float32)
            gath[j, r, cols] = (x * scale[:, cols] * (g * jax.nn.sigmoid(g))).astype(jnp.bfloat16)
        over_x(c).start()
        over_c(c).start()
        return carry

    lax.fori_loop(0, chunks, final, 0)

    def pass_on(c, carry):
        over_x(c).wait()
        over_d(c).start()
        return carry

    lax.fori_loop(0, chunks, pass_on, 0)

    def project(c, carry):
        over_c(c).wait()
        over_d(c).wait()
        r = at(c)
        acc = jnp.dot(gath[0, r, :], weight[0:width, :], preferred_element_type=jnp.float32)
        for p in range(1, 4):
            acc = acc + jnp.dot(
                gath[p, r, :], weight[p * width : (p + 1) * width, :],
                preferred_element_type=jnp.float32,
            )
        out[r, :] = acc.astype(jnp.bfloat16)
        return carry

    lax.fori_loop(0, chunks, project, 0)


def mixer(n, raw, qdec, switch, state, decay, scale, weight):
    rows, width = raw.shape
    heads = width // HEAD
    chunks = 4
    vm = pl.BlockSpec(memory_space=VMEM)
    return pl.pallas_call(
        functools.partial(mixer_kernel, n, chunks),
        name="mixer",
        out_shape=jax.ShapeDtypeStruct((rows, weight.shape[1]), jnp.bfloat16),
        in_specs=[vm] * 7,
        out_specs=vm,
        scratch_shapes=[
            VMEM((n, heads, HEAD, HEAD), jnp.bfloat16),
            VMEM((n, 8, width), jnp.float32),
            VMEM((4, rows, width), jnp.bfloat16),
            VMEM((heads, HEAD, HEAD), jnp.float32),
        ]
        + [DMA((n,))] * 4
        + [DMA((chunks,))] * 6,
        compiler_params=pltpu.CompilerParams(
            collective_id=1, has_side_effects=True, vmem_limit_bytes=48 * 2**20
        ),
        cost_estimate=pl.CostEstimate(
            flops=10**9, bytes_accessed=60 * 10**6, transcendentals=10**6
        ),
    )(raw, qdec, switch, state, decay, scale, weight)


def return_kernel(
    n, part,
    out,
    acc, sendb, recvb, fin, asend0, arecv0, asend1, arecv1, bsend, brecv, rsend, rrecv,
):
    i, j, mate, cross = places()
    mate_cross = (mate + 2) % 4
    greet(n, i, j, mate, cross)

    def to_mate(s, near):
        k = xor(i, s, n)
        if near:
            return remote(part.at[mate, k], acc.at[0, s], asend0.at[s], arecv0.at[s], (i, mate))
        return remote(part.at[mate_cross, k], acc.at[1, s], asend1.at[s], arecv1.at[s], (i, mate))

    def to_cross(s):
        return remote(sendb.at[s], recvb.at[s], bsend.at[s], brecv.at[s], (i, cross))

    def home(s):
        k = xor(i, s, n)
        return remote(fin.at[s], out.at[i], rsend.at[s], rrecv.at[s], (k, j))

    def home_in(s):
        k = xor(i, s, n)
        return remote(fin.at[s], out.at[k], rsend.at[s], rrecv.at[s], (k, j))

    def first(t, c):
        s = n - 1 - t
        to_mate(s, False).start()
        to_mate(s, True).start()
        return c

    lax.fori_loop(0, n, first, 0)

    def second(t, c):
        s = n - 1 - t
        k = xor(i, s, n)
        to_mate(s, False).wait()
        x = part[cross, k].astype(jnp.float32) + acc[1, s].astype(jnp.float32)
        sendb[s] = x.astype(jnp.bfloat16)
        to_cross(s).start()
        return c

    lax.fori_loop(0, n, second, 0)

    def total(s):
        k = xor(i, s, n)
        to_mate(s, True).wait()
        to_cross(s).wait()
        x = part[j, k].astype(jnp.float32) + acc[0, s].astype(jnp.float32)
        return (x + recvb[s].astype(jnp.float32)).astype(jnp.bfloat16)

    def third(t, c):
        s = n - 1 - t
        fin[s] = total(s)
        home(s).start()
        return c

    lax.fori_loop(0, n - 1, third, 0)
    out[i] = total(0)

    def fourth(s, c):
        home(s).wait_send()
        home_in(s).wait_recv()
        return c

    lax.fori_loop(1, n, fourth, 0)


def give_back(n, part):
    shape = part.shape[1:]
    vm = pl.BlockSpec(memory_space=VMEM)
    return pl.pallas_call(
        functools.partial(return_kernel, n),
        name="give_back",
        out_shape=jax.ShapeDtypeStruct(shape, jnp.bfloat16),
        in_specs=[vm],
        out_specs=vm,
        scratch_shapes=[
            VMEM((2,) + shape, jnp.bfloat16),
            VMEM(shape, jnp.bfloat16),
            VMEM(shape, jnp.bfloat16),
            VMEM(shape, jnp.bfloat16),
        ]
        + [DMA((n,))] * 8,
        compiler_params=pltpu.CompilerParams(
            collective_id=2, has_side_effects=True, vmem_limit_bytes=48 * 2**20
        ),
        cost_estimate=pl.CostEstimate(
            flops=10**8, bytes_accessed=150 * 10**6, transcendentals=0
        ),
    )(part)


def rms_scale(values, gain):
    return values * lax.rsqrt(jnp.mean(values * values, axis=-1, keepdims=True) + NORM_EPS) * gain


def clamped_unit(gate, upward):
    glued = jnp.minimum(gate, CLAMP_LIMIT)
    linear = jnp.clip(upward, -CLAMP_LIMIT, CLAMP_LIMIT)
    return glued * jax.nn.sigmoid(SWISH_ALPHA * glued) * (linear + 1.0)


def slot_hits(routes, experts, capacity):
    tokens, top = routes.shape
    ids = jnp.arange(experts, dtype=jnp.int32)
    onehot = (routes[:, :, None] == ids).astype(jnp.float32)
    named = jnp.sum(onehot, axis=1)
    earlier = jnp.tril(jnp.ones((tokens, tokens), jnp.float32), -1)
    ahead = jnp.dot(earlier, named, preferred_element_type=jnp.float32)
    rank = jnp.sum(onehot * ahead[:, None, :], axis=2).astype(jnp.int32)
    slots = routes * capacity + rank
    return slots[:, :, None] == jnp.arange(experts * capacity, dtype=jnp.int32)


def shards(
    state_probe_logits,
    retention_logits,
    state_source_entries,
    state_result_switch_logits,
    retention_bound_margin,
    extra_fading_amount,
    state_result_scale,
    state_result_matrix,
    second_slice_tokens,
    specialist_assignment,
    selected_specialist_share,
    leading_scale_vector,
    trailing_scale_vector,
    specialist_switch_matrix,
    specialist_widen_matrix,
    specialist_contract_matrix,
):
    n = lax.axis_size("ep")
    experts = specialist_switch_matrix.shape[0] * n
    top_count = specialist_assignment.shape[1]
    capacity = 2 * TOK_DEV * top_count // experts
    first = lax.axis_index("tp") * TOK_DEV
    own_route = lax.dynamic_slice_in_dim(specialist_assignment, first, TOK_DEV, 0)
    own_weight = lax.dynamic_slice_in_dim(selected_specialist_share, first, TOK_DEV, 0)
    own_rows = lax.dynamic_slice_in_dim(second_slice_tokens, first, TOK_DEV, 0)
    normed = rms_scale(own_rows.astype(jnp.float32), leading_scale_vector).astype(jnp.bfloat16)
    hits = slot_hits(own_route, experts, capacity)
    pick = jnp.any(hits, axis=1).astype(jnp.bfloat16)
    packed = lax.dot_general(pick, normed, TN, preferred_element_type=jnp.float32)
    packed = packed.astype(jnp.bfloat16).reshape(n, capacity, -1)

    portion, raw, qdec, state, decay = dispatch(
        n,
        packed,
        state_probe_logits,
        retention_logits,
        state_source_entries,
        retention_bound_margin[None, :],
        extra_fading_amount,
    )
    mixer_out = mixer(
        n,
        raw,
        qdec,
        state_result_switch_logits,
        state,
        decay,
        state_result_scale[None, :],
        state_result_matrix,
    )

    rows = portion.reshape(-1, portion.shape[3])
    gate = jnp.dot(rows, specialist_switch_matrix[0], preferred_element_type=jnp.float32)
    upward = jnp.dot(rows, specialist_widen_matrix[0], preferred_element_type=jnp.float32)
    activated = clamped_unit(gate, upward).astype(jnp.bfloat16)
    parts = jnp.dot(
        activated, specialist_contract_matrix[0], preferred_element_type=jnp.float32
    ).astype(jnp.bfloat16)
    returned = give_back(n, parts.reshape(portion.shape))

    flat = returned.reshape(-1, returned.shape[2])
    spread = jnp.sum(jnp.where(hits, own_weight[:, :, None], 0.0), axis=1)
    high = spread.astype(jnp.bfloat16)
    low = (spread - high.astype(jnp.float32)).astype(jnp.bfloat16)
    combined = jnp.dot(high, flat, preferred_element_type=jnp.float32) + jnp.dot(
        low, flat, preferred_element_type=jnp.float32
    )
    moe_out = rms_scale(combined, trailing_scale_vector).astype(jnp.bfloat16)
    return (mixer_out, moe_out)


def solution(mesh):
    return jax.shard_map(
        shards,
        mesh=mesh,
        in_specs=(
            P("ep", "tp"),
            P("ep", "tp"),
            P("ep", "tp"),
            P("ep", "tp"),
            P("tp"),
            P("ep", "tp"),
            P("tp"),
            P(None, "tp"),
            P("ep", None),
            P("ep", None),
            P("ep", None),
            P(),
            P(),
            P("ep", None, "tp"),
            P("ep", None, "tp"),
            P("ep", "tp", None),
        ),
        out_specs=(P("ep", "tp"), P(("ep", "tp"), None)),
        check_vma=False,
    )
```

time: 321 us -> 215 us (0.67)
  Pallas kernels: 0 us -> 180 us
  blocking collectives: 110 us -> 0 us
  waiting for transfers between devices: 89.8 us -> 0 us
  other arithmetic: 40.6 us -> 3.18 us
  between operations: 14.2 us -> 0.89 us
  matrix products: 36.9 us -> 23.8 us
  local copies, waits for them, and re-layouts: 19.3 us -> 6.57 us
  starting transfers between devices: 8.79 us -> 0 us
    pallas_call x0 -> x3, Pallas kernels: none -> 180 us  [the longest x1 82.5 us: dispatch(): pl.pallas_call(functools.partial(dispatch_kernel, n), name='dispatch', ou...]
    all_gather x2 -> x0, waiting for transfers between devices: 80.3 us -> none  [the longest x1 57.2 us: shards(): lax.all_gather(arrived.reshape(-1, arrived.shape[2]), 'tp', axis=0, tiled...]
    all_to_all x1 -> x0, blocking collectives: 55.4 us -> none  [shards(): lax.all_to_all(packed, 'ep', split_axis=0, concat_axis=0, tiled=True)]
    all_gather x2 -> x0, blocking collectives: 54.2 us -> none  [carried_in(): lax.all_gather(a.astype(kind), axis)]
    add x17 -> x2, other arithmetic: 16.5 us -> 0.7 us  [the longest x1 0.69 us: slot_hits(): slots = routes * capacity + rank]
    dot_general x7 -> x6, matrix products: 30.1 us -> 17 us  [the longest x1 7.03 us: shards(): jnp.dot(rows, specialist_switch_matrix[0], preferred_element_type=jnp.flo...]
    dynamic_update_slice x16 -> x0, other arithmetic: 10.6 us -> none  [shards(): lax.scan(advance, jnp.zeros((groups_each_device, HEAD, HEAD), jnp.float32...]
    all_to_all x1 -> x0, waiting for transfers between devices: 9.41 us -> none  [shards(): lax.all_to_all(finished, 'ep', split_axis=0, concat_axis=0, tiled=True)]
  transfers between devices with their start and end apart: 4 -> 0, of which waited for: 3 -> 0; matrix products, arithmetic and copies ran while one was open for 17% -> 0% of each run, Pallas kernels for 0% -> 0%
where the time goes in v1:
time: 215 us; the launch traced here: 214 us
  Pallas kernels  180 us (84%)
  matrix products  23.8 us (11%)
  local copies, waits for them, and re-layouts  6.57 us (3%)
  other arithmetic  3.18 us (1%)
    pallas_call x1, Pallas kernels, dispatch(): pl.pallas_call(functools.partial(dispatch_kernel, n), name='dispatch', ou...  82.5 us
    pallas_call x1, Pallas kernels, give_back(): pl.pallas_call(functools.partial(return_kernel, n), name='give_back', out...  70.1 us
    pallas_call x1, Pallas kernels, mixer(): pl.pallas_call(functools.partial(mixer_kernel, n, chunks), name='mixer',...  27.1 us
    dot_general x1, matrix products, shards(): jnp.dot(rows, specialist_switch_matrix[0], preferred_element_type=jnp.flo...  7.03 us
    dot_general x1, matrix products, shards(): jnp.dot(activated, specialist_contract_matrix[0], preferred_element_type=...  6.78 us
    dot_general x1, matrix products, shards(): jnp.dot(rows, specialist_widen_matrix[0], preferred_element_type=jnp.floa...  5.6 us
    unnamed x32, local copies, waits for them, and re-layouts  5.05 us

profile of v1, /device:TPU:0, one launch (start us, length us, event | category | flops | bytes accessed | tf_op | source)
XLA Modules:
  0.0 214.1 jit_solution(12768005000414889635)
XLA Ops:
  0.6 0.0 copy-start
  0.6 0.0 copy-start.3
  0.7 0.0 copy-start.7
  0.7 0.0 copy-start.9
  0.7 0.8 constant_dynamic-slice_fusion.1
  1.5 0.2 fusion.15
  1.8 0.7 convert_add_fusion
  2.5 0.1 fusion.10
  2.6 1.2 fusion.4
  3.8 3.2 %convolution_convert_fusion.1 = bf16[512,2048]{1,0:T(8,128)(2,1)} fusion(pred[128,512]{1,0:T(8,128)(4,1)S(1)} %fusion.10, f32[2048]{0:T(1024)} %param.27, f32[128]{0:T(128)S(1)} %add_rsqrt_fusion.1, bf16[512,2048]{1,0:T(8,128)(2,1)} %param.24, s32[]{:T(128)S(6)} %select_n.13), kind=kOutput, calls=%fused_computation.2 | convolution fusion | flops 270532608 | bytes 2695684 | tf_op jit(solution)/shard_map/dot_general | solution.py:485
  7.0 0.0 copy-done.9
  7.0 0.2 copy.23.extra
  7.3 0.0 copy-done.3
  7.3 0.0 copy-done.7
  7.3 0.0 copy-start.1
  7.3 1.6 copy-done.1
  8.9 0.0 copy-start.4
  8.9 1.0 copy-done.4
  9.9 0.0 copy-start.5
  9.9 1.0 copy-done.5
  11.0 0.0 copy-start.2
  11.0 0.0 copy-start.6
  11.0 0.0 copy-start.8
  11.0 82.5 %dispatch.1 = (bf16[4,8,64,2048]{3,2,1,0:T(8,128)(2,1)}, f32[1024,256]{1,0:T(8,128)S(1)}, bf16[1024,256]{1,0:T(8,128)(2,1)S(1)}, bf16[2,128,128]{2,1,0:T(8,128)(2,1)S(1)}, f32[8,256]{1,0:T(8,128)S(1)}) custom-call(bf16[8,64,2048]{2,1,0:T(8,128)(2,1)S(1)} %bitcast.24, bf16[1024,256]{1,0:T(8,128)(2,1)S(1)} %copy-done.3, bf16[1024,256]{1,0:T(8,128)(2,1)S(1)} %copy-done.4, ...), custom_call_target="tpu_custom_call" | custom-call | flops 1000000000 | bytes 150000000 | tf_op jit(solution)/shard_map/dispatch/pallas_call | solution.py:189
  93.5 0.0 copy-done.2
  93.5 0.0 copy-done.6
  93.5 0.0 copy-done.8
  93.5 0.0 slice-start
  93.5 27.1 %mixer.1 = bf16[1024,512]{1,0:T(8,128)(2,1)S(1)} custom-call(f32[1024,256]{1,0:T(8,128)S(1)} %get-tuple-element.7.raw, bf16[1024,256]{1,0:T(8,128)(2,1)S(1)} %get-tuple-element.8.qdec, bf16[1024,256]{1,0:T(8,128)(2,1)S(1)} %copy-done.6, bf16[2,128,128]{2,1,0:T(8,128)(2,1)S(1)} %get-tuple-element.9.state, f32[8,256]{1,0:T(8,128)S(1)} %get-tuple-element.10.decay, ...), custom_call_target="tpu_custom_call" | custom-call | flops 1000000000 | bytes 60000000 | tf_op jit(solution)/shard_map/mixer/pallas_call | solution.py:317
  120.6 0.0 copy-done.11
  120.6 0.0 slice-start.1
  120.6 0.0 copy-start.12
  120.6 7.0 %fusion.2 = f32[2048,512]{1,0:T(8,128)S(1)} fusion(bf16[2048,2048]{1,0:T(8,128)(2,1)} %bitcast.28, bf16[1,2048,512]{2,1,0:T(8,128)(2,1)S(1)} %copy-done.11), kind=kOutput, calls=%fused_computation.6 | convolution fusion | flops 4294967296 | bytes 14680064 | tf_op jit(solution)/shard_map/dot_general | solution.py:509
  127.7 0.0 slice-done
  127.7 0.0 slice-done.1
  127.7 0.0 copy-done.12
  127.7 5.6 %multiply_convert_fusion = bf16[2048,512]{1,0:T(8,128)(2,1)S(1)} fusion(f32[2048,512]{1,0:T(8,128)S(1)} %fusion.2, bf16[2048,2048]{1,0:T(8,128)(2,1)S(1)} %bitcast.31, bf16[1,2048,512]{2,1,0:T(8,128)(2,1)S(1)} %copy-done.12), kind=kOutput, calls=%fused_computation.1 | convolution fusion | flops 4305453056 | bytes 16777216 | tf_op jit(solution)/shard_map/dot_general | solution.py:510
  133.3 0.0 copy-done
  133.3 6.8 %convolution_convert_fusion = bf16[2048,2048]{1,0:T(8,128)(2,1)} fusion(bf16[2048,512]{1,0:T(8,128)(2,1)S(1)} %multiply_convert_fusion, bf16[1,512,2048]{2,1,0:T(8,128)(2,1)S(1)} %copy-done), kind=kOutput, calls=%fused_computation | convolution fusion | flops 4299161600 | bytes 12582912 | tf_op jit(solution)/shard_map/dot_general | solution.py:512
  140.1 70.1 %give_back.1 = bf16[8,64,2048]{2,1,0:T(8,128)(2,1)S(1)} custom-call(bf16[4,8,64,2048]{3,2,1,0:T(8,128)(2,1)} %bitcast.27), custom_call_target="tpu_custom_call" | custom-call | flops 100000000 | bytes 150000000 | tf_op jit(solution)/shard_map/give_back/pallas_call | solution.py:412
  210.2 0.7 constant_dynamic-slice_fusion
  210.9 0.1 select_reduce_fusion
  211.1 0.4 fusion.13
  211.5 0.0 copy-start.10
  211.5 0.5 multiply_reduce_fusion
  212.1 0.1 copy-done.10
  212.2 0.9 multiply_convert_fusion.1
  213.2 1.0 copy.25
  (7 shorter events, 0.1 us)
Async XLA Ops:
  0.6 132.7 %copy-start = (bf16[1,512,2048]{2,1,0:T(8,128)(2,1)S(1)}, bf16[1,512,2048]{2,1,0:T(8,128)(2,1)}, u32[]{:S(2)}) copy-start(bf16[1,512,2048]{2,1,0:T(8,128)(2,1)} %param.31) | copy-start | bytes 6291460
  0.6 6.6 %copy-start.3 = (bf16[1024,256]{1,0:T(8,128)(2,1)S(1)}, bf16[1024,256]{1,0:T(8,128)(2,1)}, u32[]{:S(2)}) copy-start(bf16[1024,256]{1,0:T(8,128)(2,1)} %probe.1) | copy-start | bytes 1572868
  0.7 6.6 %copy-start.7 = (f32[256]{0:T(256)S(1)}, f32[256]{0:T(256)}, u32[]{:S(2)}) copy-start(f32[256]{0:T(256)} %param.20) | copy-start | bytes 3076
  0.7 6.4 %copy-start.9 = (f32[1024,2]{0,1:T(2,128)S(1)}, f32[1024,2]{0,1:T(2,128)}, u32[]{:S(2)}) copy-start(f32[1024,2]{0,1:T(2,128)} %param.21) | copy-start | bytes 24580
  7.3 1.6 copy-start.1
  8.9 1.0 copy-start.4
  9.9 1.0 copy-start.5
  11.0 82.5 %copy-start.2 = (bf16[1024,512]{1,0:T(8,128)(2,1)S(1)}, bf16[1024,512]{1,0:T(8,128)(2,1)}, u32[]{:S(2)}) copy-start(bf16[1024,512]{1,0:T(8,128)(2,1)} %weight.1) | copy-start | bytes 3145732
  11.0 82.5 %copy-start.6 = (bf16[1024,256]{1,0:T(8,128)(2,1)S(1)}, bf16[1024,256]{1,0:T(8,128)(2,1)}, u32[]{:S(2)}) copy-start(bf16[1024,256]{1,0:T(8,128)(2,1)} %switch.1) | copy-start | bytes 1572868
  11.0 82.5 %copy-start.8 = (f32[256]{0:T(256)S(1)}, f32[256]{0:T(256)}, u32[]{:S(2)}) copy-start(f32[256]{0:T(256)} %param.22) | copy-start | bytes 3076
  11.0 109.6 %copy-start.11 = (bf16[1,2048,512]{2,1,0:T(8,128)(2,1)S(1)}, bf16[1,2048,512]{2,1,0:T(8,128)(2,1)}, u32[]{:S(2)}) copy-start(bf16[1,2048,512]{2,1,0:T(8,128)(2,1)} %param.29) | copy-start | bytes 6291460
  93.5 34.2 %slice-start = ((s8[8388608]{0:T(1024)(128)(4,1)}), s8[4194304]{0:T(1024)(128)(4,1)S(1)}, s32[]{:S(2)}) async-start(s8[8388608]{0:T(1024)(128)(4,1)} %bitcast.29), calls=%async_computation | async-start | bytes 8388608
  120.6 7.1 %slice-start.1 = ((s8[8388608]{0:T(1024)(128)(4,1)}), s8[4194304]{0:T(1024)(128)(4,1)S(1)}, s32[]{:S(2)}) async-start(s8[8388608]{0:T(1024)(128)(4,1)} %bitcast.29), calls=%async_computation.1 | async-start | bytes 8388608
  120.6 7.1 %copy-start.12 = (bf16[1,2048,512]{2,1,0:T(8,128)(2,1)S(1)}, bf16[1,2048,512]{2,1,0:T(8,128)(2,1)}, u32[]{:S(2)}) copy-start(bf16[1,2048,512]{2,1,0:T(8,128)(2,1)} %param.30) | copy-start | bytes 6291460
  211.5 0.7 copy-start.10

commit v2 on v1

--- a/solution.py
+++ b/solution.py
@@ -96,84 +96,166 @@
         running[:, cols] = running[:, cols] + last
 
 
-def dispatch_kernel(
-    n, packed, probe, ret, val, margin, extra,
-    out, raw, qdec, state_out, running,
-    state, asend, arecv, xsend, xrecv, csend, crecv, dsend, drecv, own_sem,
+def moe_kernel(
+    n, packed, probe, ret, val, margin, extra, gate_hbm, up_hbm, down_hbm,
+    raw, qdec, state_out, running, back,
+    state, rows, part, gate_w, up_w, down_w, acc, sendb, recvb, fin,
+    asend, arecv, xsend, xrecv, csend, crecv, dsend, drecv, own_sem, weight_sem,
+    esend0, erecv0, esend1, erecv1, bsend, brecv, rsend, rrecv,
 ):
     i, j, mate, cross = places()
+    mate_cross = (mate + 2) % 4
     spans = probe.shape[0] // SPAN
+    capacity, features = packed.shape[1], packed.shape[2]
+    loads = [
+        pltpu.make_async_copy(src, dst, weight_sem.at[w])
+        for w, (src, dst) in enumerate(((gate_hbm, gate_w), (up_hbm, up_w), (down_hbm, down_w)))
+    ]
+    for load in loads:
+        load.start()
     greet(n, i, j, mate, cross)
 
     def direct(s):
         k = xor(i, s, n)
-        return remote(packed.at[k], out.at[j, i], asend.at[s], arecv.at[s], (k, j))
+        return remote(packed.at[k], rows.at[i, j], asend.at[s], arecv.at[s], (k, j))
 
     def over_x(src, s):
         k = xor(i, s, n)
-        return remote(src, out.at[j, k], xsend.at[s], xrecv.at[s], (i, cross))
+        return remote(src, rows.at[k, j], xsend.at[s], xrecv.at[s], (i, cross))
 
     def over_c(src, s):
         k = xor(i, s, n)
-        return remote(src, out.at[j, k], csend.at[s], crecv.at[s], (i, mate))
+        return remote(src, rows.at[k, j], csend.at[s], crecv.at[s], (i, mate))
 
     def over_d(s):
         k = xor(i, s, n)
-        return remote(out.at[cross, k], out.at[cross, k], dsend.at[s], drecv.at[s], (i, mate))
+        return remote(rows.at[k, cross], rows.at[k, cross], dsend.at[s], drecv.at[s], (i, mate))
+
+    def to_mate(s, near):
+        k = xor(i, s, n)
+        if near:
+            return remote(part.at[k, mate], acc.at[0, k], esend0.at[s], erecv0.at[s], (i, mate))
+        return remote(
+            part.at[k, mate_cross], acc.at[1, k], esend1.at[s], erecv1.at[s], (i, mate)
+        )
+
+    def to_cross(s):
+        return remote(sendb.at[s], recvb.at[s], bsend.at[s], brecv.at[s], (i, cross))
+
+    def home(s):
+        k = xor(i, s, n)
+        return remote(fin.at[s], back.at[i], rsend.at[s], rrecv.at[s], (k, j))
+
+    def home_in(s):
+        k = xor(i, s, n)
+        return remote(fin.at[s], back.at[k], rsend.at[s], rrecv.at[s], (k, j))
 
     def start_direct(t, c):
         direct(n - 1 - t).start()
         return c
 
-    lax.fori_loop(0, n - 1, start_direct, 0)
-    own = pltpu.make_async_copy(packed.at[i], out.at[j, i], own_sem)
+    direct(1).start()
+    lax.fori_loop(0, n - 2, start_direct, 0)
+    own = pltpu.make_async_copy(packed.at[i], rows.at[i, j], own_sem)
     own.start()
     over_x(packed.at[i], 0).start()
     over_c(packed.at[i], 0).start()
     state[...] = jnp.zeros_like(state)
     running[...] = jnp.zeros_like(running)
 
+    def order(t):
+        return ((t + n - 1) // n) * (1 + (n - t) % (n - 1))
+
     def span(t):
         span_step(t, probe, ret, val, margin, extra, raw, qdec, state, running)
 
-    def serve(t, c):
+    def serve(t):
+        s = order(t)
+        k = xor(i, s, n)
+        direct(s).wait_recv()
+        over_x(rows.at[k, j], s).start()
+        over_c(rows.at[k, j], s).start()
+
+    def work(t):
+        s = order(t)
+        k = xor(i, s, n)
+        over_c(packed.at[i], s).wait_recv()
+        over_d(s).wait_recv()
+        x = rows[k].reshape(4 * capacity, features)
+        gate = jnp.dot(x, gate_w[...], preferred_element_type=jnp.float32)
+        upward = jnp.dot(x, up_w[...], preferred_element_type=jnp.float32)
+        act = clamped_unit(gate, upward).astype(jnp.bfloat16)
+        step = 512
+        for f in range(0, features, step):
+            y = jnp.dot(act, down_w[:, f : f + step], preferred_element_type=jnp.float32)
+            part[k, :, :, f : f + step] = y.astype(jnp.bfloat16).reshape(4, capacity, step)
+        to_mate(s, False).start()
+        to_mate(s, True).start()
+
+    def first_sum(t):
+        s = order(t)
+        k = xor(i, s, n)
+        to_mate(s, False).wait()
+        x = part[k, cross].astype(jnp.float32) + acc[1, k].astype(jnp.float32)
+        sendb[s] = x.astype(jnp.bfloat16)
+        to_cross(s).start()
+
+    def total(s):
+        k = xor(i, s, n)
+        to_mate(s, True).wait()
+        to_cross(s).wait()
+        x = part[k, j].astype(jnp.float32) + acc[0, k].astype(jnp.float32)
+        return (x + recvb[s].astype(jnp.float32)).astype(jnp.bfloat16)
+
+    def pump(t, c):
         @pl.when(t < spans)
         def _():
             span(t)
 
-        s = n - 1 - t
-        k = xor(i, s, n)
-        direct(s).wait_recv()
-        over_x(out.at[j, k], s).start()
-        over_c(out.at[j, k], s).start()
-        before = (s + 1) % n
-        over_x(out.at[j, xor(i, before, n)], before).wait_recv()
-        over_d(before).start()
-        return c
-
-    lax.fori_loop(0, n - 1, serve, 0)
-
-    def rest(t, c):
-        span(t)
-        return c
-
-    if spans > n - 1:
-        lax.fori_loop(n - 1, spans, rest, 0)
-    over_x(packed.at[i], 1).wait_recv()
-    over_d(1).start()
+        @pl.when(t + 1 < n)
+        def _():
+            serve(t + 1)
+
+        @pl.when(t < n)
+        def _():
+            s = order(t)
+            over_x(packed.at[i], s).wait_recv()
+            over_d(s).start()
+
+        @pl.when((t >= 1) & (t < n + 1))
+        def _():
+            work(t - 1)
+
+        @pl.when((t >= 2) & (t < n + 2))
+        def _():
+            first_sum(t - 2)
+
+        @pl.when((t >= 4) & (t < n + 3))
+        def _():
+            s = order(t - 3)
+            fin[s] = total(s)
+            home(s).start()
+
+        return c
+
     own.wait()
+    for load in loads:
+        load.wait()
+    lax.fori_loop(0, max(n + 3, spans), pump, 0)
+    back[i] = total(0)
 
     def finish(s, c):
         over_x(packed.at[i], s).wait_send()
         over_c(packed.at[i], s).wait_send()
-        over_c(packed.at[i], s).wait_recv()
-        over_d(s).wait()
+        over_d(s).wait_send()
         return c
 
     lax.fori_loop(0, n, finish, 0)
 
     def finish_direct(s, c):
         direct(s).wait_send()
+        home(s).wait_send()
+        home_in(s).wait_recv()
         return c
 
     lax.fori_loop(1, n, finish_direct, 0)
@@ -181,31 +263,47 @@
         state_out[h] = state[h].astype(jnp.bfloat16)
 
 
-def dispatch(n, packed, probe, ret, val, margin, extra):
-    rows, width = probe.shape
+def moe(n, packed, probe, ret, val, margin, extra, gate_w, up_w, down_w):
+    length, width = probe.shape
     heads = width // HEAD
     vm = pl.BlockSpec(memory_space=VMEM)
     hbm = pl.BlockSpec(memory_space=pl.ANY)
+    chunk = packed.shape[1:]
+    bf = jnp.bfloat16
     return pl.pallas_call(
-        functools.partial(dispatch_kernel, n),
-        name="dispatch",
+        functools.partial(moe_kernel, n),
+        name="moe",
         out_shape=(
-            jax.ShapeDtypeStruct((4,) + packed.shape, jnp.bfloat16),
-            jax.ShapeDtypeStruct((rows, width), jnp.float32),
-            jax.ShapeDtypeStruct((rows, width), jnp.bfloat16),
-            jax.ShapeDtypeStruct((heads, HEAD, HEAD), jnp.bfloat16),
+            jax.ShapeDtypeStruct((length, width), jnp.float32),
+            jax.ShapeDtypeStruct((length, width), bf),
+            jax.ShapeDtypeStruct((heads, HEAD, HEAD), bf),
             jax.ShapeDtypeStruct((8, width), jnp.float32),
+            jax.ShapeDtypeStruct(packed.shape, bf),
         ),
-        in_specs=[vm] * 6,
-        out_specs=(hbm, vm, vm, vm, vm),
-        scratch_shapes=[VMEM((heads, HEAD, HEAD), jnp.float32)] + [DMA((n,))] * 8 + [DMA],
+        in_specs=[vm] * 6 + [hbm] * 3,
+        out_specs=(vm,) * 5,
+        scratch_shapes=[
+            VMEM((heads, HEAD, HEAD), jnp.float32),
+            VMEM((n, 4) + chunk, bf),
+            VMEM((n, 4) + chunk, bf),
+            VMEM(gate_w.shape, bf),
+            VMEM(up_w.shape, bf),
+            VMEM(down_w.shape, bf),
+            VMEM((2, n) + chunk, bf),
+            VMEM((n,) + chunk, bf),
+            VMEM((n,) + chunk, bf),
+            VMEM((n,) + chunk, bf),
+        ]
+        + [DMA((n,))] * 8
+        + [DMA, DMA((3,))]
+        + [DMA((n,))] * 8,
         compiler_params=pltpu.CompilerParams(
-            collective_id=0, has_side_effects=True, vmem_limit_bytes=48 * 2**20
+            collective_id=0, has_side_effects=True, vmem_limit_bytes=60 * 2**20
         ),
         cost_estimate=pl.CostEstimate(
-            flops=10**9, bytes_accessed=150 * 10**6, transcendentals=10**6
+            flops=10**10, bytes_accessed=200 * 10**6, transcendentals=10**6
         ),
-    )(packed, probe, ret, val, margin, extra)
+    )(packed, probe, ret, val, margin, extra, gate_w, up_w, down_w)
 
 
 def mixer_kernel(
@@ -335,100 +433,6 @@
             flops=10**9, bytes_accessed=60 * 10**6, transcendentals=10**6
         ),
     )(raw, qdec, switch, state, decay, scale, weight)
-
-
-def return_kernel(
-    n, part,
-    out,
-    acc, sendb, recvb, fin, asend0, arecv0, asend1, arecv1, bsend, brecv, rsend, rrecv,
-):
-    i, j, mate, cross = places()
-    mate_cross = (mate + 2) % 4
-    greet(n, i, j, mate, cross)
-
-    def to_mate(s, near):
-        k = xor(i, s, n)
-        if near:
-            return remote(part.at[mate, k], acc.at[0, s], asend0.at[s], arecv0.at[s], (i, mate))
-        return remote(part.at[mate_cross, k], acc.at[1, s], asend1.at[s], arecv1.at[s], (i, mate))
-
-    def to_cross(s):
-        return remote(sendb.at[s], recvb.at[s], bsend.at[s], brecv.at[s], (i, cross))
-
-    def home(s):
-        k = xor(i, s, n)
-        return remote(fin.at[s], out.at[i], rsend.at[s], rrecv.at[s], (k, j))
-
-    def home_in(s):
-        k = xor(i, s, n)
-        return remote(fin.at[s], out.at[k], rsend.at[s], rrecv.at[s], (k, j))
-
-    def first(t, c):
-        s = n - 1 - t
-        to_mate(s, False).start()
-        to_mate(s, True).start()
-        return c
-
-    lax.fori_loop(0, n, first, 0)
-
-    def second(t, c):
-        s = n - 1 - t
-        k = xor(i, s, n)
-        to_mate(s, False).wait()
-        x = part[cross, k].astype(jnp.float32) + acc[1, s].astype(jnp.float32)
-        sendb[s] = x.astype(jnp.bfloat16)
-        to_cross(s).start()
-        return c
-
-    lax.fori_loop(0, n, second, 0)
-
-    def total(s):
-        k = xor(i, s, n)
-        to_mate(s, True).wait()
-        to_cross(s).wait()
-        x = part[j, k].astype(jnp.float32) + acc[0, s].astype(jnp.float32)
-        return (x + recvb[s].astype(jnp.float32)).astype(jnp.bfloat16)
-
-    def third(t, c):
-        s = n - 1 - t
-        fin[s] = total(s)
-        home(s).start()
-        return c
-
-    lax.fori_loop(0, n - 1, third, 0)
-    out[i] = total(0)
-
-    def fourth(s, c):
-        home(s).wait_send()
-        home_in(s).wait_recv()
-        return c
-
-    lax.fori_loop(1, n, fourth, 0)
-
-
-def give_back(n, part):
-    shape = part.shape[1:]
-    vm = pl.BlockSpec(memory_space=VMEM)
-    return pl.pallas_call(
-        functools.partial(return_kernel, n),
-        name="give_back",
-        out_shape=jax.ShapeDtypeStruct(shape, jnp.bfloat16),
-        in_specs=[vm],
-        out_specs=vm,
-        scratch_shapes=[
-            VMEM((2,) + shape, jnp.bfloat16),
-            VMEM(shape, jnp.bfloat16),
-            VMEM(shape, jnp.bfloat16),
-            VMEM(shape, jnp.bfloat16),
-        ]
-        + [DMA((n,))] * 8,
-        compiler_params=pltpu.CompilerParams(
-            collective_id=2, has_side_effects=True, vmem_limit_bytes=48 * 2**20
-        ),
-        cost_estimate=pl.CostEstimate(
-            flops=10**8, bytes_accessed=150 * 10**6, transcendentals=0
-        ),
-    )(part)
 
 
 def rms_scale(values, gain):
@@ -485,7 +489,7 @@
     packed = lax.dot_general(pick, normed, TN, preferred_element_type=jnp.float32)
     packed = packed.astype(jnp.bfloat16).reshape(n, capacity, -1)
 
-    portion, raw, qdec, state, decay = dispatch(
+    raw, qdec, state, decay, returned = moe(
         n,
         packed,
         state_probe_logits,
@@ -493,6 +497,9 @@
         state_source_entries,
         retention_bound_margin[None, :],
         extra_fading_amount,
+        specialist_switch_matrix[0],
+        specialist_widen_matrix[0],
+        specialist_contract_matrix[0],
     )
     mixer_out = mixer(
         n,
@@ -504,15 +511,6 @@
         state_result_scale[None, :],
         state_result_matrix,
     )
-
-    rows = portion.reshape(-1, portion.shape[3])
-    gate = jnp.dot(rows, specialist_switch_matrix[0], preferred_element_type=jnp.float32)
-    upward = jnp.dot(rows, specialist_widen_matrix[0], preferred_element_type=jnp.float32)
-    activated = clamped_unit(gate, upward).astype(jnp.bfloat16)
-    parts = jnp.dot(
-        activated, specialist_contract_matrix[0], preferred_element_type=jnp.float32
-    ).astype(jnp.bfloat16)
-    returned = give_back(n, parts.reshape(portion.shape))
 
     flat = returned.reshape(-1, returned.shape[2])
     spread = jnp.sum(jnp.where(hits, own_weight[:, :, None], 0.0), axis=1)

time: 215 us -> 180 us (0.84)
  matrix products: 23.8 us -> 6.14 us
  Pallas kernels: 180 us -> 165 us
  local copies, waits for them, and re-layouts: 6.57 us -> 3.18 us
    dot_general x3 -> x0, matrix products: 19.4 us -> none  [the longest x1 7.03 us: shards(): jnp.dot(rows, specialist_switch_matrix[0], preferred_element_type=jnp.flo...]
    pallas_call x2 -> x1, Pallas kernels: 153 us -> 138 us  [moe(): pl.pallas_call(functools.partial(moe_kernel, n), name='moe', out_shape=(j...]
    unnamed x32 -> x24, local copies, waits for them, and re-layouts: 5.05 us -> 2.48 us
where the time goes in v2:
time: 180 us; the launch traced here: 178 us
  Pallas kernels  165 us (92%)
  matrix products  6.14 us (3%)
  local copies, waits for them, and re-layouts  3.18 us (2%)
  other arithmetic  3.18 us (2%)
    pallas_call x1, Pallas kernels, moe(): pl.pallas_call(functools.partial(moe_kernel, n), name='moe', out_shape=(j...  138 us
    pallas_call x1, Pallas kernels, mixer(): pl.pallas_call(functools.partial(mixer_kernel, n, chunks), name='mixer',...  27.1 us

profile of v2, /device:TPU:0, one launch (start us, length us, event | category | flops | bytes accessed | tf_op | source)
XLA Modules:
  0.0 178.1 jit_solution(9073756842983463268)
XLA Ops:
  0.6 0.0 copy-start
  0.6 0.0 copy-start.9
  0.7 0.7 constant_dynamic-slice_fusion.1
  1.4 0.2 fusion.11
  1.6 0.7 convert_add_fusion
  2.3 0.1 fusion.6
  2.4 1.2 fusion
  3.7 3.2 %convolution_convert_fusion = bf16[512,2048]{1,0:T(8,128)(2,1)} fusion(pred[128,512]{1,0:T(8,128)(4,1)S(1)} %fusion.6, f32[2048]{0:T(1024)} %param.27, f32[128]{0:T(128)S(1)} %add_rsqrt_fusion.1, bf16[512,2048]{1,0:T(8,128)(2,1)} %param.24, s32[]{:T(128)S(6)} %select_n.13), kind=kOutput, calls=%fused_computation | convolution fusion | flops 270532608 | bytes 2695684 | tf_op jit(solution)/shard_map/dot_general | solution.py:489
  6.9 0.0 copy-done.9
  6.9 1.0 copy.23.extra
  7.9 137.7 %moe.1 = (f32[1024,256]{1,0:T(8,128)}, bf16[1024,256]{1,0:T(8,128)(2,1)}, bf16[2,128,128]{2,1,0:T(8,128)(2,1)}, f32[8,256]{1,0:T(8,128)}, bf16[8,64,2048]{2,1,0:T(8,128)(2,1)}) custom-call(bf16[8,64,2048]{2,1,0:T(8,128)(2,1)} %bitcast.14, bf16[1024,256]{1,0:T(8,128)(2,1)} %probe.1, bf16[1024,256]{1,0:T(8,128)(2,1)} %ret.1, bf16[1024,256]{1,0:T(8,128)(2,1)} %val.1, ...), custom_call_target="tpu_custom_call" | custom-call | flops 10000000000 | bytes 200000000 | tf_op jit(solution)/shard_map/moe/pallas_call | solution.py:273
  145.6 0.0 copy-start.8
  145.6 0.0 copy-done
  145.6 0.1 select_reduce_fusion
  145.8 2.2 %fusion.9 = f32[128,2048]{1,0:T(8,128)S(1)} fusion(bf16[512,2048]{1,0:T(8,128)(2,1)} %bitcast.12, f32[128,512]{1,0:T(8,128)S(1)} %select_reduce_fusion), kind=kOutput, calls=%fused_computation.17 | convolution fusion | flops 268500992 | bytes 3407872 | tf_op jit(solution)/shard_map/dot_general | solution.py:519
  147.9 0.0 copy-done.8
  148.0 0.0 copy-start.10
  148.0 0.0 copy-start.1
  148.0 0.0 copy-start.2
  148.0 0.0 copy-start.3
  148.0 0.0 copy-start.4
  148.0 0.0 copy-start.5
  148.0 0.0 copy-start.6
  148.0 0.0 copy-start.7
  148.0 0.6 multiply_reduce_fusion
  148.6 0.0 copy-done.10
  148.7 0.9 multiply_convert_fusion
  149.6 0.0 copy-done.1
  149.6 0.0 copy-done.2
  149.6 0.0 copy-done.3
  149.7 0.3 copy-done.4
  150.0 0.0 copy-done.5
  150.0 0.0 copy-done.6
  150.0 0.0 copy-done.7
  150.0 27.1 %mixer.1 = bf16[1024,512]{1,0:T(8,128)(2,1)S(1)} custom-call(f32[1024,256]{1,0:T(8,128)S(1)} %copy-done.2, bf16[1024,256]{1,0:T(8,128)(2,1)S(1)} %copy-done.4, bf16[1024,256]{1,0:T(8,128)(2,1)S(1)} %copy-done.3, bf16[2,128,128]{2,1,0:T(8,128)(2,1)S(1)} %copy-done.5, f32[8,256]{1,0:T(8,128)S(1)} %copy-done.6, f32[1,256]{1,0:T(1,128)S(1)} %bitcast.11, ...), custom_call_target="tpu_custom_call" | custom-call | flops 1000000000 | bytes 60000000 | tf_op jit(solution)/shard_map/mixer/pallas_call | solution.py:415
  177.1 1.0 copy.25
  (6 shorter events, 0.1 us)
Async XLA Ops:
  0.6 145.0 %copy-start = (f32[512,2]{0,1:T(2,128)S(1)}, f32[512,2]{0,1:T(2,128)}, u32[]{:S(2)}) copy-start(f32[512,2]{0,1:T(2,128)} %param.26) | copy-start | bytes 12292
  0.6 6.2 %copy-start.9 = (f32[1024,2]{0,1:T(2,128)S(1)}, f32[1024,2]{0,1:T(2,128)}, u32[]{:S(2)}) copy-start(f32[1024,2]{0,1:T(2,128)} %param.21) | copy-start | bytes 24580
  145.6 2.4 %copy-start.8 = (bf16[8,64,2048]{2,1,0:T(8,128)(2,1)S(1)}, bf16[8,64,2048]{2,1,0:T(8,128)(2,1)}, u32[]{:S(2)}) copy-start(bf16[8,64,2048]{2,1,0:T(8,128)(2,1)} %get-tuple-element.11) | copy-start | bytes 6291460
  148.0 0.7 copy-start.10
  148.0 1.6 copy-start.1
  148.0 1.6 copy-start.2
  148.0 1.7 copy-start.3
  148.0 2.0 %copy-start.4 = (bf16[1024,256]{1,0:T(8,128)(2,1)S(1)}, bf16[1024,256]{1,0:T(8,128)(2,1)}, u32[]{:S(2)}) copy-start(bf16[1024,256]{1,0:T(8,128)(2,1)} %get-tuple-element.8.qdec) | copy-start | bytes 1572868
  148.0 2.0 %copy-start.5 = (bf16[2,128,128]{2,1,0:T(8,128)(2,1)S(1)}, bf16[2,128,128]{2,1,0:T(8,128)(2,1)}, u32[]{:S(2)}) copy-start(bf16[2,128,128]{2,1,0:T(8,128)(2,1)} %get-tuple-element.9.state) | copy-start | bytes 196612
  148.0 2.0 %copy-start.6 = (f32[8,256]{1,0:T(8,128)S(1)}, f32[8,256]{1,0:T(8,128)}, u32[]{:S(2)}) copy-start(f32[8,256]{1,0:T(8,128)} %get-tuple-element.10.decay) | copy-start | bytes 24580
  148.0 2.0 %copy-start.7 = (f32[256]{0:T(256)S(1)}, f32[256]{0:T(256)}, u32[]{:S(2)}) copy-start(f32[256]{0:T(256)} %param.22) | copy-start | bytes 3076
